TPU v7x, 32 devices: a whole 2x2x4 slice. The times are simulated.
32 devices in a mesh: grp: 2 (over y), fs: 4 (over z), tp: 4 (over x, core).
Axes of the slice: x: 2, y: 2, z: 4, core: 2. Of those that a mesh axis runs over, the one named last changes fastest.
Arguments:
- tokens: bfloat16 [4096, 2048], P(('grp', 'fs', 'tp')), parts along dimension 0, may hold values from -12 to 12
- norm_gain: float32 [2048], replicated, may hold values from 0.1 to 1.9
- w_in: bfloat16 [2048, 8192], P('fs', 'tp'), may hold values from -0.125 to 0.125
- w_out: bfloat16 [8192, 2048], P('tp', 'fs'), may hold values from -0.0625 to 0.0625
Outputs:
- mixed: bfloat16 [4096, 2048], P(('grp', 'fs', 'tp')), parts along dimension 0
There are 2 independent parts, one for each index of `grp`. A program takes and returns all parts, laid end to end along the dimension named above; an argument that names none is the same for every part. Nothing has to cross between parts.
All inputs are finite; a program needn't handle non-finite values.
Results may differ from a plain program's by a relative error of at most 0.012.
Values may be sent and summed in bfloat16 or wider, within the bound.
A program may use at most 64 MiB of HBM per device.

v0:
```python
import jax
import jax.numpy as jnp
from jax import lax
from jax.sharding import PartitionSpec as P

EPS = 1e-06


def local(tokens, norm_gain, w_in, w_out):
    xf = tokens.astype(jnp.float32)
    scale = lax.rsqrt(jnp.mean(xf * xf, axis=-1, keepdims=True) + EPS)
    normed = (xf * scale * norm_gain).astype(jnp.bfloat16)
    group = lax.all_gather(normed, "tp", axis=0, tiled=True)
    pre = jnp.dot(
        group, lax.all_gather(w_in, "fs", axis=0, tiled=True), preferred_element_type=jnp.float32
    )
    hidden = jnp.square(jax.nn.relu(pre)).astype(jnp.bfloat16)
    terms = jnp.dot(
        hidden, lax.all_gather(w_out, "fs", axis=1, tiled=True), preferred_element_type=jnp.float32
    )
    summed = lax.psum_scatter(
        terms.astype(jnp.bfloat16), "tp", scatter_dimension=0, tiled=True
    ).astype(jnp.float32)
    return (xf + summed).astype(jnp.bfloat16)


def solution(mesh):
    in_specs = (P(("grp", "fs", "tp"), None), P(), P("fs", "tp"), P("tp", "fs"))
    out_specs = P(("grp", "fs", "tp"), None)
    return jax.shard_map(local, mesh=mesh, in_specs=in_specs, out_specs=out_specs, check_vma=False)
```

profile of v0, /device:TPU:0, one launch (start us, length us, event | category | flops | bytes accessed | tf_op | source)
XLA Modules:
  0.0 390.5 jit_solution(15908731586754024758)
XLA Ops:
  6.5 0.0 all-gather.4.cloned.1.call-start
  6.5 1.2 fusion
  7.8 2.0 fusion.2
  9.8 0.0 all-gather.4.cloned.1.call-update
  9.8 0.0 all-gather.6.cloned.1.call-start
  9.9 0.7 all-gather.6.cloned.1.call-update
  10.6 0.0 all-gather.8.cloned.1.call-start
  10.6 0.7 all-gather.8.cloned.1.call-update
  11.3 0.0 copy-start
  11.3 0.0 reduce-scatter.2.cloned.1.call-start
  11.4 23.9 %all-gather.4.cloned.1.call-done = bf16[512,2048]{1,0:T(8,128)(2,1)} async-done(((bf16[128,2048]{1,0:T(8,128)(2,1)}), bf16[512,2048]{1,0:T(8,128)(2,1)}) %all-gather.4.cloned.1.call-update) | async-done | bytes 2097168 | tf_op jit(solution)/shard_map/all_gather | solution.py:13
  35.3 151.2 %all-gather.6.cloned.1.call-done = bf16[2048,2048]{1,0:T(8,128)(2,1)} async-done(((bf16[512,2048]{1,0:T(8,128)(2,1)}), bf16[2048,2048]{1,0:T(8,128)(2,1)}) %all-gather.6.cloned.1.call-update) | async-done | bytes 8388624 | tf_op jit(solution)/shard_map/all_gather | solution.py:15
  186.5 149.4 %all-gather.8.cloned.1.call-done = bf16[2048,2048]{1,0:T(8,128)(2,1)} async-done(((bf16[2048,512]{1,0:T(8,128)(2,1)}), bf16[2048,2048]{1,0:T(8,128)(2,1)}) %all-gather.8.cloned.1.call-update) | async-done | bytes 8388624 | tf_op jit(solution)/shard_map/all_gather | solution.py:19
  335.9 16.5 %convolution_convert_fusion = bf16[512,2048]{1,0:T(8,128)(2,1)} fusion(bf16[2048,2048]{1,0:T(8,128)(2,1)} %all-gather.8.cloned.1.call-done, bf16[512,2048]{1,0:T(8,128)(2,1)} %all-gather.4.cloned.1.call-done, bf16[2048,2048]{1,0:T(8,128)(2,1)} %all-gather.6.cloned.1.call-done), kind=kOutput, calls=%fused_computation.1 | convolution fusion | flops 8594128896 | bytes 20971520 | tf_op jit(solution)/shard_map/dot_general | solution.py:18
  352.4 0.0 reduce-scatter.2.cloned.1.call-update
  352.4 29.5 %reduce-scatter.2.cloned.1.call-done = bf16[128,2048]{1,0:T(8,128)(2,1)} async-done(((bf16[512,2048]{1,0:T(8,128)(2,1)}), bf16[128,2048]{1,0:T(8,128)(2,1)}) %reduce-scatter.2.cloned.1.call-update) | async-done | bytes 524304 | tf_op jit(solution)/shard_map/reduce_scatter | solution.py:21
  382.0 0.0 copy-done
  382.0 2.0 fusion.3
  (1 shorter events, 0.0 us)
Async XLA Ops:
  6.5 28.7 %all-gather.4.cloned.1.call-start = ((), (), s32[]{:S(2)}) async-start(), calls=%async_computation.1 | async-start | bytes 2621440 | tf_op jit(solution)/shard_map/all_gather | solution.py:13
  9.8 176.7 %all-gather.6.cloned.1.call-start = ((), (), s32[]{:S(2)}) async-start(), calls=%async_computation.2 | async-start | bytes 10485760 | tf_op jit(solution)/shard_map/all_gather | solution.py:15
  10.6 325.3 %all-gather.8.cloned.1.call-start = ((), (), s32[]{:S(2)}) async-start(), calls=%async_computation.3 | async-start | bytes 10485760 | tf_op jit(solution)/shard_map/all_gather | solution.py:19
  11.3 370.6 %copy-start = (bf16[128,2048]{1,0:T(8,128)(2,1)S(1)}, bf16[128,2048]{1,0:T(8,128)(2,1)}, u32[]{:S(2)}) copy-start(bf16[128,2048]{1,0:T(8,128)(2,1)} %param.4) | copy-start | bytes 1572868
  11.3 370.6 %reduce-scatter.2.cloned.1.call-start = ((), (), s32[]{:S(2)}) async-start(), calls=%async_computation.4 | async-start | bytes 2621440 | tf_op jit(solution)/shard_map/reduce_scatter | solution.py:21
Sparse Core Ops, SparseCore 0:
  9.9 25.2 all-gather.3
  36.8 149.6 all-gather.5
  188.1 147.7 all-gather.7
  352.6 29.3 reduce-scatter.1
where the time goes:
time: 391 us; the launch traced here: 390 us
  waiting for transfers between devices  355 us (91%)
  matrix products  16.5 us (4%)
  between operations  13.1 us (3%)
  other arithmetic  5.23 us (1%)
    all_gather x1, waiting for transfers between devices, local(): lax.all_gather(w_in, 'fs', axis=0, tiled=True)  151 us
    all_gather x1, waiting for transfers between devices, local(): lax.all_gather(w_out, 'fs', axis=1, tiled=True)  149 us
    reduce_scatter x1, waiting for transfers between devices, local(): lax.psum_scatter(terms.astype(jnp.bfloat16), 'tp', scatter_dimension=0, t...  29.5 us
    all_gather x1, waiting for transfers between devices, local(): group = lax.all_gather(normed, 'tp', axis=0, tiled=True)  23.9 us
    dot_general x1, matrix products, local(): jnp.dot(hidden, lax.all_gather(w_out, 'fs', axis=1, tiled=True), preferre...  16.5 us
  transfers between devices with their start and end apart: 4, of which 4 were waited for; matrix products, arithmetic and copies ran while one was open for 0% of the time, Pallas kernels for 0%

commit v1 on v0

v1 whole, which is shorter than its diff:
```python
import jax
import jax.numpy as jnp
from jax import lax
from jax.sharding import PartitionSpec as P

EPS = 1e-06
PLANE = ("grp", "tp")


def local(tokens, norm_gain, w_in, w_out):
    xf = tokens.astype(jnp.float32)
    scale = lax.rsqrt(jnp.mean(xf * xf, axis=-1, keepdims=True) + EPS)
    normed = (xf * scale * norm_gain).astype(jnp.bfloat16)
    group = lax.all_gather(normed, PLANE, axis=0, tiled=True)
    half = w_in.shape[1] // lax.axis_size("grp")
    first = lax.axis_index("grp") * half
    mine_in = lax.dynamic_slice_in_dim(w_in, first, half, 1)
    mine_out = lax.dynamic_slice_in_dim(w_out, first, half, 0)
    pre = jnp.dot(
        group, lax.all_gather(mine_in, "fs", axis=0, tiled=True), preferred_element_type=jnp.float32
    )
    hidden = jnp.square(jax.nn.relu(pre)).astype(jnp.bfloat16)
    terms = jnp.dot(
        hidden, lax.all_gather(mine_out, "fs", axis=1, tiled=True), preferred_element_type=jnp.float32
    )
    summed = lax.psum_scatter(
        terms.astype(jnp.bfloat16), PLANE, scatter_dimension=0, tiled=True
    ).astype(jnp.float32)
    return (xf + summed).astype(jnp.bfloat16)


def solution(mesh):
    in_specs = (P(("grp", "fs", "tp"), None), P(), P("fs", "tp"), P("tp", "fs"))
    out_specs = P(("grp", "fs", "tp"), None)
    return jax.shard_map(local, mesh=mesh, in_specs=in_specs, out_specs=out_specs, check_vma=False)
```

time: 391 us -> 285 us (0.73)
  waiting for transfers between devices: 355 us -> 249 us
  local copies, waits for them, and re-layouts: 0.01 us -> 5 us
    all_gather x3, waiting for transfers between devices: 325 us -> 198 us  [the longest x1 80.8 us: local(): lax.all_gather(mine_out, 'fs', axis=1, tiled=True)]
    reduce_scatter x1, waiting for transfers between devices: 29.5 us -> 51.3 us  [local(): lax.psum_scatter(terms.astype(jnp.bfloat16), PLANE, scatter_dimension=0,...]
  transfers between devices with their start and end apart: 4 -> 4, of which waited for: 4 -> 4; matrix products, arithmetic and copies ran while one was open for 0% -> 1% of each run, Pallas kernels for 0% -> 0%
where the time goes in v1:
time: 285 us
  waiting for transfers between devices  249 us (87%)
  matrix products  14.4 us (5%)
  between operations  13.2 us (5%)
  local copies, waits for them, and re-layouts  5 us (2%)
  other arithmetic  3.14 us (1%)
    all_gather x1, waiting for transfers between devices, local(): lax.all_gather(mine_out, 'fs', axis=1, tiled=True)  80.8 us
    all_gather x1, waiting for transfers between devices, local(): lax.all_gather(mine_in, 'fs', axis=0, tiled=True)  79.9 us
    reduce_scatter x1, waiting for transfers between devices, local(): lax.psum_scatter(terms.astype(jnp.bfloat16), PLANE, scatter_dimension=0,...  51.3 us
    all_gather x1, waiting for transfers between devices, local(): group = lax.all_gather(normed, PLANE, axis=0, tiled=True)  37 us
    dot_general x1, matrix products, local(): jnp.dot(hidden, lax.all_gather(mine_out, 'fs', axis=1, tiled=True), prefe...  14.4 us
  transfers between devices with their start and end apart: 4, of which 4 were waited for; matrix products, arithmetic and copies ran while one was open for 1% of the time, Pallas kernels for 0%

profile of v1, /device:TPU:0, one launch (start us, length us, event | category | flops | bytes accessed | tf_op | source)
XLA Modules:
  0.0 284.9 jit_solution(4599781802018407765)
XLA Ops:
  6.5 0.0 copy-start
  6.5 0.0 copy-start.1
  6.5 0.0 copy-start.2
  6.5 0.0 all-gather.6.cloned.1.call-start
  6.6 1.6 copy-done
  8.1 1.1 constant_dynamic-slice_fusion.1
  9.3 0.0 all-gather.6.cloned.1.call-update
  9.3 0.0 all-gather.8.cloned.1.call-start
  9.3 2.3 constant_dynamic-slice_fusion
  11.6 0.0 all-gather.8.cloned.1.call-update
  11.6 0.0 all-gather.4.cloned.1.call-start
  11.7 0.0 copy-done.1
  11.7 0.2 fusion
  11.9 0.0 copy-done.2
  11.9 1.0 fusion.2
  12.9 0.0 all-gather.4.cloned.1.call-update
  12.9 0.0 reduce-scatter.2.cloned.1.call-start
  13.0 79.9 %all-gather.6.cloned.1.call-done = bf16[2048,1024]{1,0:T(8,128)(2,1)} async-done(((bf16[512,1024]{1,0:T(8,128)(2,1)}), bf16[2048,1024]{1,0:T(8,128)(2,1)}) %all-gather.6.cloned.1.call-update) | async-done | bytes 4194320 | tf_op jit(solution)/shard_map/all_gather | solution.py:20
  92.9 80.8 %all-gather.8.cloned.1.call-done = bf16[1024,2048]{1,0:T(8,128)(2,1)} async-done(((bf16[1024,512]{1,0:T(8,128)(2,1)}), bf16[1024,2048]{1,0:T(8,128)(2,1)}) %all-gather.8.cloned.1.call-update) | async-done | bytes 4194320 | tf_op jit(solution)/shard_map/all_gather | solution.py:24
  173.7 37.0 %all-gather.4.cloned.1.call-done = bf16[1024,2048]{1,0:T(8,128)(2,1)} async-done(((bf16[128,2048]{1,0:T(8,128)(2,1)}), bf16[1024,2048]{1,0:T(8,128)(2,1)}) %all-gather.4.cloned.1.call-update) | async-done | bytes 4194320 | tf_op jit(solution)/shard_map/all_gather | solution.py:14
  210.7 14.4 %convolution_convert_fusion = bf16[1024,2048]{1,0:T(8,128)(2,1)} fusion(bf16[1024,2048]{1,0:T(8,128)(2,1)} %all-gather.8.cloned.1.call-done, bf16[1024,2048]{1,0:T(8,128)(2,1)} %all-gather.4.cloned.1.call-done, bf16[2048,1024]{1,0:T(8,128)(2,1)} %all-gather.6.cloned.1.call-done), kind=kOutput, calls=%fused_computation.1 | convolution fusion | flops 8595177472 | bytes 16777216 | tf_op jit(solution)/shard_map/dot_general | solution.py:23
  225.1 0.0 reduce-scatter.2.cloned.1.call-update
  225.1 51.3 %reduce-scatter.2.cloned.1.call-done = bf16[128,2048]{1,0:T(8,128)(2,1)} async-done(((bf16[1024,2048]{1,0:T(8,128)(2,1)}), bf16[128,2048]{1,0:T(8,128)(2,1)}) %reduce-scatter.2.cloned.1.call-update) | async-done | bytes 524304 | tf_op jit(solution)/shard_map/reduce_scatter | solution.py:26
  276.4 2.0 fusion.3
  (1 shorter events, 0.0 us)
Async XLA Ops:
  6.5 1.6 copy-start
  6.5 5.2 %copy-start.1 = (bf16[128,2048]{1,0:T(8,128)(2,1)S(1)}, bf16[128,2048]{1,0:T(8,128)(2,1)}, u32[]{:S(2)}) copy-start(bf16[128,2048]{1,0:T(8,128)(2,1)} %param.4) | copy-start | bytes 1572868
  6.5 5.4 %copy-start.2 = (f32[2048]{0:T(1024)S(1)}, f32[2048]{0:T(1024)}, u32[]{:S(2)}) copy-start(f32[2048]{0:T(1024)} %param.5) | copy-start | bytes 24580
  6.5 86.4 %all-gather.6.cloned.1.call-start = ((), (), s32[]{:S(2)}) async-start(), calls=%async_computation.2 | async-start | bytes 5242880 | tf_op jit(solution)/shard_map/all_gather | solution.py:20
  9.3 164.4 %all-gather.8.cloned.1.call-start = ((), (), s32[]{:S(2)}) async-start(), calls=%async_computation.3 | async-start | bytes 5242880 | tf_op jit(solution)/shard_map/all_gather | solution.py:24
  11.6 199.1 %all-gather.4.cloned.1.call-start = ((), (), s32[]{:S(2)}) async-start(), calls=%async_computation.1 | async-start | bytes 4718592 | tf_op jit(solution)/shard_map/all_gather | solution.py:14
  12.9 263.5 %reduce-scatter.2.cloned.1.call-start = ((), (), s32[]{:S(2)}) async-start(), calls=%async_computation.4 | async-start | bytes 4718592 | tf_op jit(solution)/shard_map/reduce_scatter | solution.py:26
Sparse Core Ops, SparseCore 0:
  9.4 83.4 all-gather.5
  94.5 79.2 all-gather.7
  175.6 35.0 all-gather.3
  225.2 51.1 reduce-scatter.1

commit v2 on v0

v2 whole, which is shorter than its diff:
```python
import functools

import jax
import jax.numpy as jnp
from jax import lax
from jax.experimental import pallas as pl
from jax.experimental.pallas import tpu as pltpu
from jax.sharding import PartitionSpec as P

EPS = 1e-06
MESH = pl.DeviceIdType.MESH
CORES = 2
PLANES = 2


def remote(src, dst, send, recv, device):
    pltpu.make_async_remote_copy(
        src_ref=src, dst_ref=dst, send_sem=send, recv_sem=recv, device_id=device, device_id_type=MESH
    ).start()


def done(ref, sem):
    pltpu.make_async_copy(ref, ref, sem).wait()


def kernel(
    Y, n, X, parts, x_ref, g_ref, wi_ref, wo_ref, o_ref,
    norm, wi, wo, hid, crecv, precv, zsend, zrecv, acc,
    tok_send, tok_recv, wi_send, wi_recv, wo_send, wo_recv,
    c_send, c_recv, p_send, p_recv, z_send, z_recv,
):
    y, i, j = lax.axis_index("grp"), lax.axis_index("fs"), lax.axis_index("tp")
    x, core, zp = j // CORES, j % CORES, i % PLANES
    chips = Y * X
    chip = y * X + x
    B, D = x_ref.shape
    HU = wi.shape[1]
    Dr, Dc = wi_ref.shape[0], wo_ref.shape[1]
    W = Dc // parts
    NC = n * parts
    R = norm.shape[0]
    half = R // CORES
    pair_rows = PLANES * B

    partner = (y, i, x * CORES + 1 - core)
    zpair = (y, i + 1 - 2 * zp, j)

    def at_chip(k):
        return (k // X, i, (k % X) * CORES + core)

    def other_chip(o):
        return lax.rem(chip + o, chips)

    direction = jnp.where(i < n // 2, 1, -1)

    barrier = pltpu.get_barrier_semaphore()
    for k in range(1, n):
        pl.semaphore_signal(barrier, inc=1, device_id=(y, lax.rem(i + k, n), j), device_id_type=MESH)
    pl.semaphore_signal(barrier, inc=1, device_id=partner, device_id_type=MESH)
    for o in range(1, chips):
        pl.semaphore_signal(barrier, inc=1, device_id=at_chip(other_chip(o)), device_id_type=MESH)

    def block(c, k, z):
        return (c * chips + k) * PLANES + z

    def rows_of(b):
        return pl.ds(pl.multiple_of(b * B, B), B)

    mine = block(core, chip, zp)

    @pl.loop(0, B // 16)
    def _(r):
        rows = pl.ds(pl.multiple_of(r * 16, 16), 16)
        xf = x_ref[rows, :].astype(jnp.float32)
        scale = lax.rsqrt(jnp.mean(xf * xf, axis=-1, keepdims=True) + EPS)
        out_rows = pl.ds(pl.multiple_of(mine * B + r * 16, 16), 16)
        norm[out_rows, :] = (xf * scale * g_ref[...]).astype(jnp.bfloat16)

    pl.semaphore_wait(barrier, (n - 1) + 1 + (chips - 1))

    count = [0]

    def send_block(b, device):
        ref = norm.at[rows_of(b), :]
        remote(ref, ref, tok_send.at[count[0]], tok_recv.at[b], device)
        count[0] += 1

    send_block(mine, zpair)
    for o in range(1, chips):
        send_block(mine, at_chip(other_chip(o)))
    send_block(mine, partner)

    def in_cols(d):
        return pl.ds(pl.multiple_of(((d % PLANES) * Y + y) * HU, HU), HU)

    def in_rows(s):
        return pl.ds(pl.multiple_of(s * Dr, Dr), Dr)

    def out_cols(cid):
        return pl.ds(pl.multiple_of(cid * W, W), W)

    for k in range(1, n):
        d = lax.rem(i + n - direction * k, n)
        remote(wi_ref.at[:, in_cols(d)], wi.at[in_rows(i), :], wi_send.at[d], wi_recv.at[i], (y, d, j))
    pltpu.make_async_copy(wi_ref.at[:, in_cols(i)], wi.at[in_rows(i), :], wi_recv.at[i]).start()
    for h in range(parts):
        cid = i * parts + h
        for k in range(1, n):
            d = lax.rem(i + n - direction * k, n)
            remote(
                wo_ref.at[in_cols(d), pl.ds(h * W, W)], wo.at[:, out_cols(cid)],
                wo_send.at[d * parts + h], wo_recv.at[cid], (y, d, j),
            )
        pltpu.make_async_copy(
            wo_ref.at[in_cols(i), pl.ds(h * W, W)], wo.at[:, out_cols(cid)], wo_recv.at[cid]
        ).start()

    def arrived(b):
        done(norm.at[rows_of(b), :], tok_recv.at[b])

    paired = block(core, chip, 1 - zp)
    arrived(paired)
    for o in range(1, chips):
        send_block(paired, at_chip(other_chip(o)))
    send_block(paired, partner)
    for z in (zp, 1 - zp):
        for o in range(1, chips):
            b = block(core, other_chip(chips - o), z)
            arrived(b)
            send_block(b, partner)
    for o in range(chips):
        for z in range(PLANES):
            arrived(block(1 - core, other_chip(o), z))

    for s in range(n):
        done(wi.at[in_rows(s), :], wi_recv.at[s])

    TR = min(256, half)

    @pl.loop(0, R // TR)
    def _(r):
        rows = pl.ds(pl.multiple_of(r * TR, TR), TR)
        pre = jnp.dot(norm[rows, :], wi[...], preferred_element_type=jnp.float32)
        hid[rows, :] = jnp.square(jnp.maximum(pre, 0.0)).astype(jnp.bfloat16)

    for q in range(count[0]):
        done(norm.at[rows_of(0), :], tok_send.at[q])

    kept, given = core * half, (1 - core) * half

    def chunk(t):
        s = lax.rem(i + n + direction * (t % n), n)
        return s * parts + t // n

    def multiply(first, cols):
        @pl.loop(0, half // TR)
        def _(r):
            rows = pl.ds(pl.multiple_of(first + r * TR, TR), TR)
            norm[rows, cols] = jnp.dot(
                hid[rows, :], wo[:, cols], preferred_element_type=jnp.float32
            ).astype(jnp.bfloat16)

    def chip_rows(base, k):
        return pl.ds(pl.multiple_of(base + k * pair_rows, pair_rows), pair_rows)

    def fold(k, cols):
        rows = chip_rows(kept, k)
        norm[rows, cols] = (
            norm[rows, cols].astype(jnp.float32) + crecv[chip_rows(0, k), cols].astype(jnp.float32)
        ).astype(jnp.bfloat16)

    @pl.loop(0, NC + 2)
    def _(t):
        @pl.when(t < NC)
        def _():
            cid = chunk(t)
            cols = out_cols(cid)
            done(wo.at[:, cols], wo_recv.at[cid])
            multiply(given, cols)
            remote(
                norm.at[pl.ds(pl.multiple_of(given, half), half), cols], crecv.at[:, cols],
                c_send.at[cid], c_recv.at[cid], partner,
            )
            multiply(kept, cols)
            done(crecv.at[:, cols], c_recv.at[cid])
            for o in range(1, chips):
                k = other_chip(o)
                fold(k, cols)
                remote(
                    norm.at[chip_rows(kept, k), cols], precv.at[chip, :, cols],
                    p_send.at[cid * chips + k], p_recv.at[cid * chips + chip], at_chip(k),
                )
            fold(chip, cols)

        @pl.when(t >= 2)
        def _():
            cid = chunk(t - 2)
            cols = out_cols(cid)
            for o in range(1, chips):
                k = other_chip(o)
                done(precv.at[k, :, cols], p_recv.at[cid * chips + k])

            def total(z):
                inner = pl.ds(pl.multiple_of(z * B, B), B)
                first = kept + chip * pair_rows + z * B
                value = norm[pl.ds(pl.multiple_of(first, B), B), cols].astype(jnp.float32)
                for o in range(1, chips):
                    value += precv[other_chip(o), inner, cols].astype(jnp.float32)
                return value

            zsend[:, cols] = total(1 - zp).astype(jnp.bfloat16)
            remote(zsend.at[:, cols], zrecv.at[:, cols], z_send.at[cid], z_recv.at[cid], zpair)
            acc[:, cols] = total(zp)

    @pl.loop(0, NC)
    def _(t):
        cid = chunk(t)
        cols = out_cols(cid)
        done(zrecv.at[:, cols], z_recv.at[cid])
        total = acc[:, cols] + zrecv[:, cols].astype(jnp.float32)
        o_ref[:, cols] = (x_ref[:, cols].astype(jnp.float32) + total).astype(jnp.bfloat16)

    for k in range(1, n):
        d = lax.rem(i + k, n)
        done(wi.at[in_rows(0), :], wi_send.at[d])
        for h in range(parts):
            done(wo.at[:, out_cols(0)], wo_send.at[d * parts + h])

    @pl.loop(0, NC)
    def _(cid):
        cols = out_cols(cid)
        done(crecv.at[:, cols], c_send.at[cid])
        done(zsend.at[:, cols], z_send.at[cid])
        for o in range(1, chips):
            k = other_chip(o)
            done(precv.at[k, :, cols], p_send.at[cid * chips + k])


def solution(mesh):
    Y, n, T = mesh.shape["grp"], mesh.shape["fs"], mesh.shape["tp"]
    X = T // CORES
    chips = Y * X

    def local(tokens, norm_gain, w_in, w_out):
        B, D = tokens.shape
        HU = w_in.shape[1] // (PLANES * Y)
        Dc = w_out.shape[1]
        parts = 2 if Dc % 256 == 0 else 1
        NC = n * parts
        R = CORES * chips * PLANES * B
        sends = 1 + chips + chips + PLANES * (chips - 1)
        bf16 = jnp.bfloat16
        dma = pltpu.SemaphoreType.DMA
        vmem = pl.BlockSpec(memory_space=pltpu.VMEM)
        hbm = pl.BlockSpec(memory_space=pl.ANY)
        return pl.pallas_call(
            functools.partial(kernel, Y, n, X, parts),
            out_shape=jax.ShapeDtypeStruct((B, D), bf16),
            in_specs=[vmem, vmem, hbm, hbm],
            out_specs=vmem,
            scratch_shapes=[
                pltpu.VMEM((R, D), bf16),
                pltpu.VMEM((D, HU), bf16),
                pltpu.VMEM((HU, D), bf16),
                pltpu.VMEM((R, HU), bf16),
                pltpu.VMEM((R // CORES, D), bf16),
                pltpu.VMEM((chips, PLANES * B, D), bf16),
                pltpu.VMEM((B, D), bf16),
                pltpu.VMEM((B, D), bf16),
                pltpu.VMEM((B, D), jnp.float32),
                dma((sends,)), dma((CORES * chips * PLANES,)),
                dma((n,)), dma((n,)),
                dma((NC,)), dma((NC,)),
                dma((NC,)), dma((NC,)),
                dma((NC * chips,)), dma((NC * chips,)),
                dma((NC,)), dma((NC,)),
            ],
            compiler_params=pltpu.CompilerParams(
                collective_id=0, has_side_effects=True, vmem_limit_bytes=60 * 1024 * 1024
            ),
        )(tokens, norm_gain.reshape(1, D), w_in, w_out)

    in_specs = (P(("grp", "fs", "tp"), None), P(), P("fs", "tp"), P("tp", "fs"))
    out_specs = P(("grp", "fs", "tp"), None)
    return jax.shard_map(local, mesh=mesh, in_specs=in_specs, out_specs=out_specs, check_vma=False)
```

time: 391 us -> 139 us (0.36)
  waiting for transfers between devices: 355 us -> 0 us
  Pallas kernels: 0 us -> 137 us
  matrix products: 16.5 us -> 0 us
  between operations: 13.1 us -> 0.01 us
  other arithmetic: 5.23 us -> 0 us
    all_gather x3 -> x0, waiting for transfers between devices: 325 us -> none  [the longest x1 151 us: local(): lax.all_gather(w_in, 'fs', axis=0, tiled=True)]
    pallas_call x0 -> x1, Pallas kernels: none -> 137 us  [local(): pl.pallas_call(functools.partial(kernel, Y, n, X, parts), out_shape=jax.S...]
    reduce_scatter x1 -> x0, waiting for transfers between devices: 29.5 us -> none  [local(): lax.psum_scatter(terms.astype(jnp.bfloat16), 'tp', scatter_dimension=0, t...]
    dot_general x1 -> x0, matrix products: 16.5 us -> none  [local(): jnp.dot(hidden, lax.all_gather(w_out, 'fs', axis=1, tiled=True), preferre...]
    convert_element_type x2 -> x0, other arithmetic: 3.99 us -> none  [the longest x1 2.03 us: local(): normed = (xf * scale * norm_gain).astype(jnp.bfloat16)]
  transfers between devices with their start and end apart: 4 -> 0, of which waited for: 4 -> 0; matrix products, arithmetic and copies ran while one was open for 0% -> 0% of each run, Pallas kernels for 0% -> 0%
where the time goes in v2:
time: 139 us
  Pallas kernels  137 us (99%)
  local copies, waits for them, and re-layouts  1.88 us (1%)
    pallas_call x1, Pallas kernels, local(): pl.pallas_call(functools.partial(kernel, Y, n, X, parts), out_shape=jax.S...  137 us

profile of v2, /device:TPU:0, one launch (start us, length us, event | category | flops | bytes accessed | tf_op | source)
XLA Modules:
  0.0 138.8 jit_solution(11796307215080072237)
XLA Ops:
  0.0 136.9 %shard_map.46 = bf16[128,2048]{1,0:T(8,128)(2,1)} custom-call(bf16[128,2048]{1,0:T(8,128)(2,1)} %x_ref.1, f32[1,2048]{1,0:T(1,128)} %bitcast.1, bf16[512,2048]{1,0:T(8,128)(2,1)} %wi_ref.1, bf16[2048,512]{1,0:T(8,128)(2,1)} %wo_ref.1), custom_call_target="tpu_custom_call" | custom-call | tf_op jit(solution)/shard_map/pallas_call | solution.py:256
  136.9 1.9 %copy.6 = bf16[128,2048]{1,0:T(8,128)(2,1)} copy(bf16[128,2048]{1,0:T(8,128)(2,1)} %shard_map.46) | data formatting | bytes 1048576

commit v3 on v2

--- a/solution.py
+++ b/solution.py
@@ -99,18 +99,29 @@
     def out_cols(cid):
         return pl.ds(pl.multiple_of(cid * W, W), W)
 
-    for k in range(1, n):
-        d = lax.rem(i + n - direction * k, n)
+    near = i + 1 - 2 * zp
+
+    def to_planes(send):
+        for k in range(1, n):
+            d = lax.rem(i + n + direction * k, n)
+            pl.when(d != near)(functools.partial(send, d))
+        send(near)
+
+    def send_in(d):
         remote(wi_ref.at[:, in_cols(d)], wi.at[in_rows(i), :], wi_send.at[d], wi_recv.at[i], (y, d, j))
+
+    def send_out(h, d):
+        cid = i * parts + h
+        remote(
+            wo_ref.at[in_cols(d), pl.ds(h * W, W)], wo.at[:, out_cols(cid)],
+            wo_send.at[d * parts + h], wo_recv.at[cid], (y, d, j),
+        )
+
+    to_planes(send_in)
     pltpu.make_async_copy(wi_ref.at[:, in_cols(i)], wi.at[in_rows(i), :], wi_recv.at[i]).start()
     for h in range(parts):
+        to_planes(functools.partial(send_out, h))
         cid = i * parts + h
-        for k in range(1, n):
-            d = lax.rem(i + n - direction * k, n)
-            remote(
-                wo_ref.at[in_cols(d), pl.ds(h * W, W)], wo.at[:, out_cols(cid)],
-                wo_send.at[d * parts + h], wo_recv.at[cid], (y, d, j),
-            )
         pltpu.make_async_copy(
             wo_ref.at[in_cols(i), pl.ds(h * W, W)], wo.at[:, out_cols(cid)], wo_recv.at[cid]
         ).start()
@@ -245,7 +256,7 @@
         B, D = tokens.shape
         HU = w_in.shape[1] // (PLANES * Y)
         Dc = w_out.shape[1]
-        parts = 2 if Dc % 256 == 0 else 1
+        parts = Dc // 128
         NC = n * parts
         R = CORES * chips * PLANES * B
         sends = 1 + chips + chips + PLANES * (chips - 1)

time: 139 us -> 128 us (0.921)
  Pallas kernels: 137 us -> 126 us
    pallas_call x1, Pallas kernels: 137 us -> 126 us  [local(): pl.pallas_call(functools.partial(kernel, Y, n, X, parts), out_shape=jax.S...]
where the time goes in v3:
time: 128 us
  Pallas kernels  126 us (98%)
  local copies, waits for them, and re-layouts  1.88 us (1%)
    pallas_call x1, Pallas kernels, local(): pl.pallas_call(functools.partial(kernel, Y, n, X, parts), out_shape=jax.S...  126 us

profile of v3, /device:TPU:0, one launch (start us, length us, event | category | flops | bytes accessed | tf_op | source)
XLA Modules:
  0.0 128.0 jit_solution(6057753380366257568)
XLA Ops:
  0.0 126.1 %shard_map.46 = bf16[128,2048]{1,0:T(8,128)(2,1)} custom-call(bf16[128,2048]{1,0:T(8,128)(2,1)} %x_ref.1, f32[1,2048]{1,0:T(1,128)} %bitcast.1, bf16[512,2048]{1,0:T(8,128)(2,1)} %wi_ref.1, bf16[2048,512]{1,0:T(8,128)(2,1)} %wo_ref.1), custom_call_target="tpu_custom_call" | custom-call | tf_op jit(solution)/shard_map/pallas_call | solution.py:267
  126.1 1.9 %copy.6 = bf16[128,2048]{1,0:T(8,128)(2,1)} copy(bf16[128,2048]{1,0:T(8,128)(2,1)} %shard_map.46) | data formatting | bytes 1048576
